TPU v7x, 32 devices: a whole 2x2x4 slice. The times are simulated.
32 devices in a mesh: sp: 4 (over z), tp: 4 (over y, x), dp: 2 (over core).
Axes of the slice: x: 2, y: 2, z: 4, core: 2. Of those that a mesh axis runs over, the one named last changes fastest.
Arguments:
- latent: bfloat16 [2, 3072, 2048], P('dp', ('sp', 'tp')), may hold values from -3 to 3
- cond: bfloat16 [2, 2048], P('dp', 'sp'), may hold values from -6 to 6
- cond_ctx: bfloat16 [2048], P('sp'), may hold values from -6 to 6
- context: bfloat16 [2, 512, 2048], P('dp', 'sp'), may hold values from -6 to 6
- norm_gain: bfloat16 [2048], replicated, may hold values from 0.099609375 to 1.8984375
- mod_shift: bfloat16 [2048, 2048], P('sp', 'tp'), may hold values from -0.125 to 0.125
- mod_scale: bfloat16 [2048, 2048], P('sp', 'tp'), may hold values from -0.125 to 0.125
- mod_gate: bfloat16 [2048, 2048], P('sp', 'tp'), may hold values from -0.125 to 0.125
- w_query: bfloat16 [2048, 1024], P(None, 'tp'), may hold values from -0.125 to 0.125
- w_key: bfloat16 [2048, 256], P(None, 'tp'), may hold values from -0.125 to 0.125
- w_value: bfloat16 [2048, 256], P(None, 'tp'), may hold values from -0.125 to 0.125
- q_gain: bfloat16 [64], replicated, may hold values from 1 to 5.5
- k_gain: bfloat16 [64], replicated, may hold values from 1 to 5.5
- ctx_lift: float32 [16], P('tp'), may hold values from 1 to 3
- w_out: bfloat16 [1024, 2048], replicated, may hold values from -1.5 to 1.5
Outputs:
- mixed: bfloat16 [2, 3072, 2048], P('dp', ('sp', 'tp'))
All inputs are finite; a program needn't handle non-finite values.
Results may differ from a plain program's by a relative error of at most 0.009.
The roundings to bfloat16 on the way count: a program that leaves them out, or rounds other values in their place, can miss the bound.
Values may be sent and summed in bfloat16 or wider, within the bound.
A program may use at most 64 MiB of HBM per device.

v0:
```python
import jax
import jax.numpy as jnp
from jax import lax
from jax.sharding import PartitionSpec as P

HD = 64
GRID_W = 128
EPS = 1e-06
THETA = 10000.0


def modulate(row_block, gain_vec, shift_rows, scale_rows):
    values = row_block.astype(jnp.float32)
    normed = (
        values
        * lax.rsqrt(jnp.mean(values * values, axis=-1, keepdims=True) + EPS)
        * gain_vec.astype(jnp.float32)
    )
    return (normed * (1.0 + scale_rows) + shift_rows).astype(jnp.bfloat16)


def head_norm(raw_proj, gain_vec):
    samples, tokens, width = raw_proj.shape
    pieces = raw_proj.reshape(samples, tokens, width // HD, HD)
    normed = (
        pieces
        * lax.rsqrt(jnp.mean(pieces * pieces, axis=-1, keepdims=True) + EPS)
        * gain_vec.astype(jnp.float32)
    )
    return normed.transpose(0, 2, 1, 3)


def rotate(vector, positions):
    pairs_count = vector.shape[-1] // 4
    grid_row = (positions // GRID_W).astype(jnp.float32)
    grid_col = (positions % GRID_W).astype(jnp.float32)
    inverse = THETA ** (-jnp.arange(pairs_count, dtype=jnp.float32) / pairs_count)
    angles = jnp.concatenate([grid_row[:, None] * inverse, grid_col[:, None] * inverse], axis=-1)
    cosine = jnp.cos(angles)
    sine_val = jnp.sin(angles)
    first_half = vector[..., 0::2]
    second_half = vector[..., 1::2]
    turned = jnp.stack(
        [
            first_half * cosine - second_half * sine_val,
            first_half * sine_val + second_half * cosine,
        ],
        axis=-1,
    )
    return turned.reshape(vector.shape)


def split_heads(rows):
    samples, tokens, width = rows.shape
    return rows.reshape(samples, tokens, width // HD, HD).transpose(0, 2, 1, 3)


def on_device(
    latent,
    cond,
    cond_ctx,
    context,
    norm_gain,
    mod_shift,
    mod_scale,
    mod_gate,
    w_query,
    w_key,
    w_value,
    q_gain,
    k_gain,
    ctx_lift,
    w_out,
):
    samples = latent.shape[0]
    active = jax.nn.silu(
        jnp.concatenate([cond, cond_ctx[None, :]], axis=0).astype(jnp.float32)
    ).astype(jnp.bfloat16)
    partial_mods = tuple(
        (
            jnp.dot(active, weight, preferred_element_type=jnp.float32)
            for weight in (mod_shift, mod_scale, mod_gate)
        )
    )
    summed = lax.psum(partial_mods, "sp")
    shift_rows, scale_rows, gate_rows = lax.all_gather(summed, "tp", axis=1, tiled=True)
    modulated = modulate(
        latent, norm_gain, shift_rows[:samples, None, :], scale_rows[:samples, None, :]
    )
    ctx_mod = modulate(context, norm_gain, shift_rows[samples], scale_rows[samples])
    q_width = w_query.shape[1]
    k_width = w_key.shape[1]
    w_joint = jnp.concatenate([w_query, w_key, w_value], axis=1)
    projected = jnp.einsum(
        "srd,dc->src",
        lax.all_gather(modulated, "tp", axis=1, tiled=True),
        w_joint,
        preferred_element_type=jnp.float32,
    )
    tokens = projected.shape[1]
    k_heads = k_width // HD
    group_size = q_width // k_width
    positions = lax.axis_index("sp") * tokens + jnp.arange(tokens, dtype=jnp.int32)
    queries = rotate(head_norm(projected[..., :q_width], q_gain), positions).astype(jnp.bfloat16)
    queries = queries.reshape(samples, k_heads, group_size, tokens, HD)
    key_rows = rotate(
        head_norm(projected[..., q_width : q_width + k_width], k_gain), positions
    ).astype(jnp.bfloat16)
    value_rows = split_heads(projected[..., q_width + k_width :].astype(jnp.bfloat16))
    ctx_proj = jnp.einsum(
        "srd,dc->src", ctx_mod, w_joint[:, q_width:], preferred_element_type=jnp.float32
    )
    ctx_keys = head_norm(ctx_proj[..., :k_width], k_gain).astype(jnp.bfloat16)
    ctx_values = split_heads(ctx_proj[..., k_width:].astype(jnp.bfloat16))
    lift_table = ctx_lift.reshape(1, k_heads, group_size, 1, 1)
    factor = HD ** (-0.5)

    def absorb(state_now, key_block, value_block, score_lift):
        best_old, weight_sum, accumulated = state_now
        scores = (
            jnp.einsum("skgtd,skrd->skgtr", queries, key_block, preferred_element_type=jnp.float32)
            * factor
            + score_lift
        )
        peak = jnp.maximum(best_old, jnp.max(scores, axis=-1))
        weights = jnp.exp(scores - peak[..., None])
        rescale = jnp.exp(best_old - peak)
        weight_sum = weight_sum * rescale + jnp.sum(weights, axis=-1)
        accumulated = accumulated * rescale[..., None] + jnp.einsum(
            "skgtr,skrd->skgtd",
            weights.astype(jnp.bfloat16),
            value_block,
            preferred_element_type=jnp.float32,
        )
        return (peak, weight_sum, accumulated)

    stat_shape = (samples, k_heads, group_size, tokens)
    state_now = (
        jnp.full(stat_shape, -1e30, jnp.float32),
        jnp.zeros(stat_shape, jnp.float32),
        jnp.zeros(stat_shape + (HD,), jnp.float32),
    )
    all_ctx_keys, all_ctx_values = (
        lax.all_gather(ctx_keys, "sp", axis=2, tiled=True),
        lax.all_gather(ctx_values, "sp", axis=2, tiled=True),
    )
    state_now = absorb(state_now, all_ctx_keys, all_ctx_values, lift_table)
    key_piece = lax.all_gather(key_rows, "sp", axis=2, tiled=True)
    value_piece = lax.all_gather(value_rows, "sp", axis=2, tiled=True)
    block_count = key_piece.shape[2] // tokens
    key_blocks = jnp.moveaxis(key_piece.reshape(samples, k_heads, block_count, tokens, HD), 2, 0)
    value_blocks = jnp.moveaxis(
        value_piece.reshape(samples, k_heads, block_count, tokens, HD), 2, 0
    )

    def step_block(carry, blocks):
        return (absorb(carry, blocks[0], blocks[1], 0.0), None)

    state_out, unused = lax.scan(step_block, state_now, (key_blocks, value_blocks))
    state_now = state_out
    best_old, weight_sum, accumulated = state_now
    attended = (accumulated / weight_sum[..., None]).astype(jnp.bfloat16)
    head_rows = attended.transpose(0, 3, 1, 2, 4).reshape(samples, tokens, q_width)
    projected_out = jnp.einsum(
        "srq,qd->srd",
        lax.all_to_all(head_rows, "tp", split_axis=1, concat_axis=2, tiled=True),
        w_out,
        preferred_element_type=jnp.float32,
    )
    return (latent.astype(jnp.float32) + gate_rows[:samples, None, :] * projected_out).astype(
        jnp.bfloat16
    )


def solution(mesh):
    placed = (
        P("dp", ("sp", "tp"), None),
        P("dp", "sp"),
        P("sp"),
        P("dp", "sp", None),
        P(),
        P("sp", "tp"),
        P("sp", "tp"),
        P("sp", "tp"),
        P(None, "tp"),
        P(None, "tp"),
        P(None, "tp"),
        P(),
        P(),
        P("tp"),
        P(),
    )
    return jax.shard_map(
        on_device,
        mesh=mesh,
        in_specs=placed,
        out_specs=P("dp", ("sp", "tp"), None),
        check_vma=False,
    )
```

profile of v0, /device:TPU:0, one launch (start us, length us, event | category | flops | bytes accessed | tf_op | source)
XLA Modules:
  0.0 190.3 jit_solution(14167755606228791362)
XLA Ops:
  6.6 0.8 broadcast_in_dim.10
  7.6 0.8 fusion.94
  8.4 1.2 fusion.96
  9.7 1.2 fusion.98
  10.9 20.5 %all-reduce = (f32[2,512]{1,0:T(2,128)S(1)}, f32[2,512]{1,0:T(2,128)S(1)}, f32[2,512]{1,0:T(2,128)S(1)}) all-reduce(f32[2,512]{1,0:T(2,128)S(1)} %fusion.94, f32[2,512]{1,0:T(2,128)S(1)} %fusion.96, f32[2,512]{1,0:T(2,128)S(1)} %fusion.98), channel_id=1, replica_groups=mesh['sp'=4,'tp'=4,'dp'=2] {'sp'}, use_global_device_ids=true, to_apply=%region_3.4 | all-reduce | flops 3072 | bytes 24576 | tf_op jit(solution)/shard_map/psum | solution.py:85
  31.4 8.2 %all_gather.25 = f32[2,2048]{1,0:T(2,128)S(1)} all-gather(f32[2,512]{1,0:T(2,128)S(1)} %get-tuple-element.88), channel_id=1, replica_groups=mesh['sp'=4,'tp'=4,'dp'=2] {'tp'}, dimensions={1}, use_global_device_ids=true | all-gather | bytes 20480 | tf_op jit(solution)/shard_map/all_gather | solution.py:86
  39.6 8.2 %all_gather.26 = f32[2,2048]{1,0:T(2,128)S(1)} all-gather(f32[2,512]{1,0:T(2,128)S(1)} %get-tuple-element.87), channel_id=1, replica_groups=mesh['sp'=4,'tp'=4,'dp'=2] {'tp'}, dimensions={1}, use_global_device_ids=true | all-gather | bytes 20480 | tf_op jit(solution)/shard_map/all_gather | solution.py:86
  47.7 0.7 convert_element_type.119
  48.4 1.4 fusion.31
  49.8 2.4 %fusion.35 = bf16[1,192,2048]{2,1,0:T(8,128)(2,1)} fusion(bf16[1,192,2048]{2,1,0:T(8,128)(2,1)} %param.17, f32[2048]{0:T(1024)S(1)} %bitcast.173, f32[2048]{0:T(1024)S(1)} %bitcast.172, f32[2048]{0:T(1024)S(1)} %convert_element_type.119, f32[192]{0:T(256)S(1)} %add_rsqrt_fusion.2), kind=kLoop, calls=%fused_computation.39 | loop fusion | flops 2359296 | bytes 1598208 | tf_op jit(solution)/shard_map/convert_element_type | solution.py:19
  53.1 0.4 convolution_bitcast_fusion
  53.6 12.0 %all_gather.28 = bf16[1,1,512,64]{2,3,1,0:T(8,128)(2,1)S(1)} all-gather(bf16[1,1,128,64]{2,3,1,0:T(8,128)(2,1)S(1)} %fusion.77), channel_id=1, replica_groups=mesh['sp'=4,'tp'=4,'dp'=2] {'sp'}, dimensions={2}, use_global_device_ids=true | all-gather | bytes 81920 | tf_op jit(solution)/shard_map/all_gather | solution.py:144
  65.7 12.6 %all-gather = bf16[1,512,64]{1,2,0:T(8,128)(2,1)} all-gather(bf16[1,128,64]{1,2,0:T(8,128)(2,1)S(1)} %slice.80), channel_id=2, replica_groups=mesh['sp'=4,'tp'=4,'dp'=2] {'sp'}, dimensions={1}, use_global_device_ids=true | all-gather | bytes 81920 | tf_op jit(solution)/shard_map/all_gather | solution.py:145
  78.3 0.7 fusion.78
  79.0 1.0 fusion.70
  80.1 13.4 %all-gather.4.cloned.1.call-done = bf16[1,768,2048]{2,1,0:T(8,128)(2,1)} async-done(((bf16[1,192,2048]{2,1,0:T(8,128)(2,1)}), bf16[1,768,2048]{2,1,0:T(8,128)(2,1)}) %all-gather.4.cloned.1.call-update) | async-done | bytes 3145744 | tf_op jit(solution)/shard_map/all_gather | solution.py:96
  93.5 3.7 %fusion.41 = f32[1,768,384]{1,2,0:T(8,128)S(1)} fusion(bf16[2048,64]{1,0:T(8,128)(2,1)S(1)} %copy.47, bf16[2048,64]{1,0:T(8,128)(2,1)S(1)} %copy.46, bf16[2048,256]{1,0:T(8,128)(2,1)} %param.25, bf16[1,768,2048]{2,1,0:T(8,128)(2,1)} %all-gather.4.cloned.1.call-done), kind=kOutput, calls=%fused_computation.45 | convolution fusion | flops 1212678144 | bytes 5898240 | tf_op jit(solution)/shard_map/srd,dc->src/dot_general | solution.py:94
  98.1 1.0 subtract_bitcast_fusion
  99.2 0.4 copy.48
  99.9 1.2 fusion.74
  101.3 14.6 %all_gather.30 = bf16[1,1,3072,64]{2,3,1,0:T(8,128)(2,1)S(1)} all-gather(bf16[1,1,768,64]{2,3,1,0:T(8,128)(2,1)S(1)} %convert_element_type.131), channel_id=1, replica_groups=mesh['sp'=4,'tp'=4,'dp'=2] {'sp'}, dimensions={2}, use_global_device_ids=true | all-gather | bytes 491520 | tf_op jit(solution)/shard_map/all_gather | solution.py:148
  115.9 1.1 fusion.21
  117.0 2.6 %copy-done.1 = f32[4,768,512]{1,2,0:T(8,128)} copy-done((f32[4,768,512]{1,2,0:T(8,128)}, f32[4,768,512]{1,2,0:T(8,128)S(1)}, u32[]{:S(2)}) %copy-start.1) | copy-done | bytes 6291480
  119.6 1.3 fusion.23
  120.9 15.5 %all-gather.1 = bf16[1,3072,64]{1,2,0:T(8,128)(2,1)S(1)} all-gather(bf16[1,768,64]{1,2,0:T(8,128)(2,1)S(1)} %slice.79), channel_id=3, replica_groups=mesh['sp'=4,'tp'=4,'dp'=2] {'sp'}, dimensions={1}, use_global_device_ids=true | all-gather | bytes 491520 | tf_op jit(solution)/shard_map/all_gather | solution.py:149
  136.8 4.3 %fusion.49 = f32[1,1,4,768,64]{3,4,2,1,0:T(8,128)S(1)} fusion(f32[4,768,512]{1,2,0:T(8,128)} %copy-done.1, f32[4,768]{1,0:T(4,128)S(1)} %get-tuple-element.106, f32[4]{0:T(128)S(1)} %copy-done.7, f32[4,768]{1,0:T(4,128)S(1)} %get-tuple-element.104, bf16[1,512,64]{1,2,0:T(8,128)(2,1)S(1)} %copy-done.6), kind=kOutput, calls=%fused_computation.49 | convolution fusion | flops 207814656 | bytes 7168016 | tf_op jit(solution)/shard_map/skgtr,skrd->skgtd/dot_general | solution.py:129
  141.0 19.7 %while.14 = (s32[]{:T(128)}, f32[1,1,4,768]{3,2,1,0:T(4,128)S(1)}, f32[1,1,4,768]{3,2,1,0:T(4,128)S(1)}, f32[1,1,4,768,64]{3,4,2,1,0:T(8,128)S(1)}, bf16[4,1,1,7...) while((s32[]{:T(128)}, f32[1,1,4,768]{3,2,1,0:T(4,128)S(1)}, ...), condition=%wide.region_13.14_spmd, body=%wide.region_10.13_spmd.sunk | while | flops 623256576 | bytes 30670940 | solution.py:159
  141.1 1.4 bitcast_reduce_fusion.2
  142.5 1.9 fusion.116
  144.4 1.6 fusion.115
  146.0 1.4 bitcast_reduce_fusion.2
  147.4 1.9 fusion.116
  149.3 1.6 fusion.115
  150.9 1.4 bitcast_reduce_fusion.2
  152.4 1.9 fusion.116
  154.3 1.6 fusion.115
  155.9 1.4 bitcast_reduce_fusion.2
  157.3 1.9 fusion.116
  159.2 1.6 fusion.115
  160.9 0.6 copy.54
  161.5 0.5 broadcast.433
  162.0 3.0 %reduce.15 = bf16[768,256]{1,0:T(8,128)(2,1)S(1)} reduce(bf16[768,1,256]{2,1,0:T(2,128)(2,1)S(1)} %bitcast.162, bf16[]{:T(256)} %broadcast.433), dimensions={1}, to_apply=%bitcast.124.reduce_sub_computation | reduce | bytes 786434
  165.0 0.8 reshape.683
  165.9 3.5 %all-to-all-start = ((bf16[4,2,24576]{2,1,0:T(2,128)(2,1)}), bf16[4,2,24576]{2,1,0:T(2,128)(2,1)S(1)}, u32[]{:S(2)}, u32[]{:S(2)}) async-start(bf16[4,2,24576]{2,1,0:T(2,128)(2,1)} %reshape.683), calls=%async_computation | async-start | bytes 786432 | tf_op jit(solution)/shard_map/all_to_all | solution.py:166
  169.4 9.1 %all_gather.24 = f32[2,2048]{1,0:T(2,128)S(1)} all-gather(f32[2,512]{1,0:T(2,128)S(1)} %get-tuple-element.89), channel_id=1, replica_groups=mesh['sp'=4,'tp'=4,'dp'=2] {'tp'}, dimensions={1}, use_global_device_ids=true | all-gather | bytes 20480 | tf_op jit(solution)/shard_map/all_gather | solution.py:86
  178.4 0.4 reshape.684
  178.9 0.3 copy.55
  179.3 4.1 %fusion.30 = bf16[1,192,2048]{2,1,0:T(8,128)(2,1)} fusion(bf16[192,1024]{1,0:T(8,128)(2,1)S(1)} %bitcast.171, bf16[1024,2048]{1,0:T(8,128)(2,1)} %param.31, bf16[1,192,2048]{2,1,0:T(8,128)(2,1)S(1)} %copy-done.2, f32[2048]{0:T(1024)S(1)} %bitcast.174), kind=kOutput, calls=%fused_computation.32 | convolution fusion | flops 806879232 | bytes 6168576 | tf_op jit(solution)/shard_map/srq,qd->srd/dot_general | solution.py:164
  (76 shorter events, 3.3 us)
Async XLA Ops:
  6.5 1.0 copy-start
  6.5 45.7 %copy-start.5 = (bf16[2048,64]{0,1:T(8,128)(2,1)S(1)}, bf16[2048,64]{0,1:T(8,128)(2,1)}, u32[]{:S(2)}) copy-start(bf16[2048,64]{0,1:T(8,128)(2,1)} %param.26) | copy-start | bytes 786436
  6.5 46.0 %copy-start.4 = (bf16[2048,64]{0,1:T(8,128)(2,1)S(1)}, bf16[2048,64]{0,1:T(8,128)(2,1)}, u32[]{:S(2)}) copy-start(bf16[2048,64]{0,1:T(8,128)(2,1)} %param.27) | copy-start | bytes 786436
  6.5 46.3 %copy-start.8 = (bf16[64]{0:T(256)(128)(2,1)S(1)}, bf16[64]{0:T(256)(128)(2,1)}, u32[]{:S(2)}) copy-start(bf16[64]{0:T(256)(128)(2,1)} %param.29) | copy-start | bytes 388
  6.5 46.3 %copy-start.9 = (bf16[64]{0:T(256)(128)(2,1)S(1)}, bf16[64]{0:T(256)(128)(2,1)}, u32[]{:S(2)}) copy-start(bf16[64]{0:T(256)(128)(2,1)} %param.28) | copy-start | bytes 388
  6.5 46.3 %copy-start.3 = (bf16[1,128,2048]{2,1,0:T(8,128)(2,1)S(1)}, bf16[1,128,2048]{2,1,0:T(8,128)(2,1)}, u32[]{:S(2)}) copy-start(bf16[1,128,2048]{2,1,0:T(8,128)(2,1)} %param.20) | copy-start | bytes 1572868
  6.6 86.9 %all-gather.4.cloned.1.call-start = ((), (), s32[]{:S(2)}) async-start(), calls=%async_computation.1 | async-start | bytes 3932160 | tf_op jit(solution)/shard_map/all_gather | solution.py:96
  97.5 18.4 %copy-start.7 = (f32[4]{0:T(128)S(1)}, f32[4]{0:T(128)}, u32[]{:S(2)}) copy-start(f32[4]{0:T(128)} %param.30) | copy-start | bytes 52
  116.9 2.7 %copy-start.1 = (f32[4,768,512]{1,2,0:T(8,128)}, f32[4,768,512]{1,2,0:T(8,128)S(1)}, u32[]{:S(2)}) copy-start(f32[4,768,512]{1,2,0:T(8,128)S(1)} %get-tuple-element.114) | copy-start | bytes 18874372
  117.0 19.8 %copy-start.6 = (bf16[1,512,64]{1,2,0:T(8,128)(2,1)S(1)}, bf16[1,512,64]{1,2,0:T(8,128)(2,1)}, u32[]{:S(2)}) copy-start(bf16[1,512,64]{1,2,0:T(8,128)(2,1)} %all-gather) | copy-start | bytes 196612
  160.8 18.5 %copy-start.2 = (bf16[1,192,2048]{2,1,0:T(8,128)(2,1)S(1)}, bf16[1,192,2048]{2,1,0:T(8,128)(2,1)}, u32[]{:S(2)}) copy-start(bf16[1,192,2048]{2,1,0:T(8,128)(2,1)} %param.17) | copy-start | bytes 2359300
  165.9 12.5 %all-to-all-start = ((bf16[4,2,24576]{2,1,0:T(2,128)(2,1)}), bf16[4,2,24576]{2,1,0:T(2,128)(2,1)S(1)}, u32[]{:S(2)}, u32[]{:S(2)}) async-start(bf16[4,2,24576]{2,1,0:T(2,128)(2,1)} %reshape.683), calls=%async_computation | async-start | bytes 786432 | tf_op jit(solution)/shard_map/all_to_all | solution.py:166
Sparse Core Ops, SparseCore 0:
  52.3 41.0 all-gather.3
where the time goes:
time: 191 us; the launch traced here: 190 us
  blocking collectives  101 us (53%)
  matrix products  30 us (16%)
  other arithmetic  20 us (10%)
  between operations  13.8 us (7%)
  waiting for transfers between devices  13.4 us (7%)
  local copies, waits for them, and re-layouts  8.75 us (5%)
  starting transfers between devices  3.5 us (2%)
    all_gather x3, blocking collectives, on_device(): lax.all_gather(summed, 'tp', axis=1, tiled=True)  25.4 us
    psum x1, blocking collectives, on_device(): summed = lax.psum(partial_mods, 'sp')  20.5 us
    all_gather x1, blocking collectives, on_device(): value_piece = lax.all_gather(value_rows, 'sp', axis=2, tiled=True)  15.5 us
    all_gather x1, blocking collectives, on_device(): key_piece = lax.all_gather(key_rows, 'sp', axis=2, tiled=True)  14.6 us
    all_gather x1, waiting for transfers between devices, on_device(): lax.all_gather(modulated, 'tp', axis=1, tiled=True)  13.4 us
    all_gather x1, blocking collectives, on_device(): lax.all_gather(ctx_values, 'sp', axis=2, tiled=True)  12.6 us
    all_gather x1, blocking collectives, on_device(): lax.all_gather(ctx_keys, 'sp', axis=2, tiled=True)  12 us
    dot_general x5, matrix products, absorb(): jnp.einsum('skgtr,skrd->skgtd', weights.astype(jnp.bfloat16), value_block...  11.7 us
  transfers between devices with their start and end apart: 2, of which 1 were waited for; matrix products, arithmetic and copies ran while one was open for 2% of the time, Pallas kernels for 0%

commit v1 on v0

--- a/solution.py
+++ b/solution.py
@@ -145,7 +145,12 @@
         lax.all_gather(ctx_values, "sp", axis=2, tiled=True),
     )
     state_now = absorb(state_now, all_ctx_keys, all_ctx_values, lift_table)
-    key_piece = lax.all_gather(key_rows, "sp", axis=2, tiled=True)
+    ring = [key_rows]
+    for hop in range(3):
+        ring.append(lax.ppermute(ring[-1], "sp", [(dev, (dev + 1) % 4) for dev in range(4)]))
+    key_piece = jnp.roll(
+        jnp.concatenate(ring[::-1], axis=2), (lax.axis_index("sp") + 1) * ring[0].shape[2], axis=2
+    )
     value_piece = lax.all_gather(value_rows, "sp", axis=2, tiled=True)
     block_count = key_piece.shape[2] // tokens
     key_blocks = jnp.moveaxis(key_piece.reshape(samples, k_heads, block_count, tokens, HD), 2, 0)

time: 191 us -> 182 us (0.953)
  blocking collectives: 101 us -> 86.5 us
  waiting for transfers between devices: 13.4 us -> 17.7 us
  starting transfers between devices: 3.5 us -> 6.58 us
    all_gather x1 -> x0, blocking collectives: 14.6 us -> none  [on_device(): key_piece = lax.all_gather(key_rows, 'sp', axis=2, tiled=True)]
    ppermute x0 -> x3, waiting for transfers between devices: none -> 4.85 us  [on_device(): lax.ppermute(ring[-1], 'sp', [(dev, (dev + 1) % 4) for dev in range(4)])]
    ppermute x0 -> x3, starting transfers between devices: none -> 3.08 us  [on_device(): lax.ppermute(ring[-1], 'sp', [(dev, (dev + 1) % 4) for dev in range(4)])]
    dot_general x5, matrix products: 11.7 us -> 8.95 us  [absorb(): jnp.einsum('skgtr,skrd->skgtd', weights.astype(jnp.bfloat16), value_block...]
    unnamed x27 -> x32, local copies, waits for them, and re-layouts: 5.28 us -> 4.5 us
  transfers between devices with their start and end apart: 2 -> 5, of which waited for: 1 -> 2; matrix products, arithmetic and copies ran while one was open for 2% -> 5% of each run, Pallas kernels for 0% -> 0%
where the time goes in v1:
time: 182 us; the launch traced here: 181 us
  blocking collectives  86.5 us (48%)
  matrix products  28.1 us (15%)
  other arithmetic  19.9 us (11%)
  waiting for transfers between devices  17.7 us (10%)
  between operations  13.9 us (8%)
  local copies, waits for them, and re-layouts  8.16 us (4%)
  starting transfers between devices  6.58 us (4%)
    all_gather x3, blocking collectives, on_device(): lax.all_gather(summed, 'tp', axis=1, tiled=True)  25.4 us
    psum x1, blocking collectives, on_device(): summed = lax.psum(partial_mods, 'sp')  20.5 us
    all_gather x1, blocking collectives, on_device(): value_piece = lax.all_gather(value_rows, 'sp', axis=2, tiled=True)  15.4 us
    all_gather x1, waiting for transfers between devices, on_device(): lax.all_gather(modulated, 'tp', axis=1, tiled=True)  12.8 us
    all_gather x1, blocking collectives, on_device(): lax.all_gather(ctx_keys, 'sp', axis=2, tiled=True)  12.6 us
    all_gather x1, blocking collectives, on_device(): lax.all_gather(ctx_values, 'sp', axis=2, tiled=True)  12.6 us
    dot_general x5, matrix products, absorb(): jnp.einsum('skgtr,skrd->skgtd', weights.astype(jnp.bfloat16), value_block...  8.95 us
    dot_general x5, matrix products, absorb(): jnp.einsum('skgtd,skrd->skgtr', queries, key_block, preferred_element_typ...  7.6 us
  transfers between devices with their start and end apart: 5, of which 2 were waited for; matrix products, arithmetic and copies ran while one was open for 5% of the time, Pallas kernels for 0%

profile of v1, /device:TPU:0, one launch (start us, length us, event | category | flops | bytes accessed | tf_op | source)
XLA Modules:
  0.0 181.0 jit_solution(13348065107260389285)
XLA Ops:
  6.6 0.8 broadcast_in_dim.10
  7.6 0.8 fusion.94
  8.4 1.2 fusion.96
  9.7 1.2 fusion.98
  10.9 20.5 %all-reduce = (f32[2,512]{1,0:T(2,128)S(1)}, f32[2,512]{1,0:T(2,128)S(1)}, f32[2,512]{1,0:T(2,128)S(1)}) all-reduce(f32[2,512]{1,0:T(2,128)S(1)} %fusion.94, f32[2,512]{1,0:T(2,128)S(1)} %fusion.96, f32[2,512]{1,0:T(2,128)S(1)} %fusion.98), channel_id=1, replica_groups=mesh['sp'=4,'tp'=4,'dp'=2] {'sp'}, use_global_device_ids=true, to_apply=%region_3.4 | all-reduce | flops 3072 | bytes 24576 | tf_op jit(solution)/shard_map/psum | solution.py:85
  31.4 8.2 %all_gather.22 = f32[2,2048]{1,0:T(2,128)S(1)} all-gather(f32[2,512]{1,0:T(2,128)S(1)} %get-tuple-element.88), channel_id=1, replica_groups=mesh['sp'=4,'tp'=4,'dp'=2] {'tp'}, dimensions={1}, use_global_device_ids=true | all-gather | bytes 20480 | tf_op jit(solution)/shard_map/all_gather | solution.py:86
  39.6 8.2 %all_gather.23 = f32[2,2048]{1,0:T(2,128)S(1)} all-gather(f32[2,512]{1,0:T(2,128)S(1)} %get-tuple-element.87), channel_id=1, replica_groups=mesh['sp'=4,'tp'=4,'dp'=2] {'tp'}, dimensions={1}, use_global_device_ids=true | all-gather | bytes 20480 | tf_op jit(solution)/shard_map/all_gather | solution.py:86
  47.7 0.7 convert_element_type.119
  48.4 1.4 fusion.31
  49.8 2.4 %fusion.35 = bf16[1,192,2048]{2,1,0:T(8,128)(2,1)} fusion(bf16[1,192,2048]{2,1,0:T(8,128)(2,1)} %param.17, f32[2048]{0:T(1024)S(1)} %bitcast.173, f32[2048]{0:T(1024)S(1)} %bitcast.172, f32[2048]{0:T(1024)S(1)} %convert_element_type.119, f32[192]{0:T(256)S(1)} %add_rsqrt_fusion.2), kind=kLoop, calls=%fused_computation.39 | loop fusion | flops 2359296 | bytes 1598208 | tf_op jit(solution)/shard_map/convert_element_type | solution.py:19
  53.1 0.4 convolution_bitcast_fusion
  53.7 12.6 %all_gather.25 = bf16[1,1,512,64]{2,3,1,0:T(8,128)(2,1)} all-gather(bf16[1,1,128,64]{2,3,1,0:T(8,128)(2,1)S(1)} %fusion.77), channel_id=1, replica_groups=mesh['sp'=4,'tp'=4,'dp'=2] {'sp'}, dimensions={2}, use_global_device_ids=true | all-gather | bytes 81920 | tf_op jit(solution)/shard_map/all_gather | solution.py:144
  66.3 12.6 %all-gather = bf16[1,512,64]{1,2,0:T(8,128)(2,1)} all-gather(bf16[1,128,64]{1,2,0:T(8,128)(2,1)S(1)} %slice.80), channel_id=2, replica_groups=mesh['sp'=4,'tp'=4,'dp'=2] {'sp'}, dimensions={1}, use_global_device_ids=true | all-gather | bytes 81920 | tf_op jit(solution)/shard_map/all_gather | solution.py:145
  78.9 0.7 fusion.78
  79.6 1.0 fusion.70
  80.7 12.8 %all-gather.4.cloned.1.call-done = bf16[1,768,2048]{2,1,0:T(8,128)(2,1)} async-done(((bf16[1,192,2048]{2,1,0:T(8,128)(2,1)}), bf16[1,768,2048]{2,1,0:T(8,128)(2,1)}) %all-gather.4.cloned.1.call-update) | async-done | bytes 3145744 | tf_op jit(solution)/shard_map/all_gather | solution.py:96
  93.5 3.7 %fusion.41 = f32[1,768,384]{1,2,0:T(8,128)S(1)} fusion(bf16[2048,64]{1,0:T(8,128)(2,1)S(1)} %copy.47, bf16[2048,64]{1,0:T(8,128)(2,1)S(1)} %copy.46, bf16[2048,256]{1,0:T(8,128)(2,1)} %param.25, bf16[1,768,2048]{2,1,0:T(8,128)(2,1)} %all-gather.4.cloned.1.call-done), kind=kOutput, calls=%fused_computation.45 | convolution fusion | flops 1212678144 | bytes 5898240 | tf_op jit(solution)/shard_map/srd,dc->src/dot_general | solution.py:94
  98.1 1.2 fusion.74
  99.4 1.5 collective-permute-start
  101.0 1.0 subtract_bitcast_fusion
  102.7 1.9 %fusion.21 = (f32[4,768]{1,0:T(4,128)S(1)}, f32[4,768,512]{1,2,0:T(8,128)S(1)}) fusion(f32[4]{0:T(128)S(1)} %copy-done.6, bf16[4,768,64]{1,2,0:T(8,128)(2,1)S(1)} %convert_element_type.125, bf16[1,1,512,64]{2,3,1,0:T(8,128)(2,1)} %all_gather.25), kind=kOutput, calls=%fused_computation.23 | convolution fusion | flops 206042112 | bytes 6762512 | tf_op jit(solution)/shard_map/skgtd,skrd->skgtr/dot_general | solution.py:121
  104.6 1.5 fusion.49
  106.0 1.3 fusion.23
  107.4 1.5 collective-permute-start.1
  109.1 4.8 %collective-permute-done.1 = bf16[1,1,768,64]{2,3,1,0:T(8,128)(2,1)} collective-permute-done((bf16[1,1,768,64]{2,3,1,0:T(8,128)(2,1)S(1)}, bf16[1,1,768,64]{2,3,1,0:T(8,128)(2,1)}, u32[]{:S(2)}, u32[]{:S(2)}) %collective-permute-start.1) | collective-permute-done | bytes 98336 | tf_op jit(solution)/shard_map/ppermute | solution.py:150
  113.9 15.4 %all-gather.1 = bf16[1,3072,64]{1,2,0:T(8,128)(2,1)S(1)} all-gather(bf16[1,768,64]{1,2,0:T(8,128)(2,1)S(1)} %slice.79), channel_id=3, replica_groups=mesh['sp'=4,'tp'=4,'dp'=2] {'sp'}, dimensions={1}, use_global_device_ids=true | all-gather | bytes 491520 | tf_op jit(solution)/shard_map/all_gather | solution.py:154
  129.7 0.9 constant_dynamic-update-slice_fusion.6
  130.7 0.9 constant_dynamic-update-slice_fusion.2
  131.8 19.7 %while.14 = (s32[]{:T(128)}, f32[1,1,4,768]{3,2,1,0:T(4,128)S(1)}, f32[1,1,4,768]{3,2,1,0:T(4,128)S(1)}, f32[1,1,4,768,64]{3,4,2,1,0:T(8,128)S(1)}, bf16[4,1,1,7...) while((s32[]{:T(128)}, f32[1,1,4,768]{3,2,1,0:T(4,128)S(1)}, ...), condition=%wide.region_13.14_spmd, body=%wide.region_10.13_spmd.sunk | while | flops 623256576 | bytes 30670940 | solution.py:164
  131.9 1.4 bitcast_reduce_fusion.2
  133.3 1.9 %fusion.116 = f32[1,1,4,768,64]{3,4,2,1,0:T(8,128)S(1)} fusion(f32[768,4,768]{2,0,1:T(8,128)S(1)} %get-tuple-element.166, f32[4,768]{1,0:T(4,128)S(1)} %bitcast.160, f32[1,1,4,768,64]{3,4,2,1,0:T(8,128)S(1)} %get-tuple-element.179, f32[4,768]{1,0:T(4,128)S(1)} %get-tuple-element.167, bf16[4,1,1,768,64]{3,4,2,1,0:T(8,128)(2,1)S(1)} %get-tuple-element.190, ...), kind=kOutput, calls=%fused_computation.7.clone.1 | convolution fusion | flops 309460992 | bytes 11132932 | tf_op jit(solution)/shard_map/while/body/eval_jaxpr/skgtr,skrd->skgtd/dot_general | solution.py:129
  135.2 1.6 fusion.115
  136.8 1.4 bitcast_reduce_fusion.2
  138.3 1.9 %fusion.116 = f32[1,1,4,768,64]{3,4,2,1,0:T(8,128)S(1)} fusion(f32[768,4,768]{2,0,1:T(8,128)S(1)} %get-tuple-element.166, f32[4,768]{1,0:T(4,128)S(1)} %bitcast.160, f32[1,1,4,768,64]{3,4,2,1,0:T(8,128)S(1)} %get-tuple-element.179, f32[4,768]{1,0:T(4,128)S(1)} %get-tuple-element.167, bf16[4,1,1,768,64]{3,4,2,1,0:T(8,128)(2,1)S(1)} %get-tuple-element.190, ...), kind=kOutput, calls=%fused_computation.7.clone.1 | convolution fusion | flops 309460992 | bytes 11132932 | tf_op jit(solution)/shard_map/while/body/eval_jaxpr/skgtr,skrd->skgtd/dot_general | solution.py:129
  140.1 1.6 fusion.115
  141.7 1.4 bitcast_reduce_fusion.2
  143.2 1.9 %fusion.116 = f32[1,1,4,768,64]{3,4,2,1,0:T(8,128)S(1)} fusion(f32[768,4,768]{2,0,1:T(8,128)S(1)} %get-tuple-element.166, f32[4,768]{1,0:T(4,128)S(1)} %bitcast.160, f32[1,1,4,768,64]{3,4,2,1,0:T(8,128)S(1)} %get-tuple-element.179, f32[4,768]{1,0:T(4,128)S(1)} %get-tuple-element.167, bf16[4,1,1,768,64]{3,4,2,1,0:T(8,128)(2,1)S(1)} %get-tuple-element.190, ...), kind=kOutput, calls=%fused_computation.7.clone.1 | convolution fusion | flops 309460992 | bytes 11132932 | tf_op jit(solution)/shard_map/while/body/eval_jaxpr/skgtr,skrd->skgtd/dot_general | solution.py:129
  145.1 1.6 fusion.115
  146.7 1.4 bitcast_reduce_fusion.2
  148.1 1.9 %fusion.116 = f32[1,1,4,768,64]{3,4,2,1,0:T(8,128)S(1)} fusion(f32[768,4,768]{2,0,1:T(8,128)S(1)} %get-tuple-element.166, f32[4,768]{1,0:T(4,128)S(1)} %bitcast.160, f32[1,1,4,768,64]{3,4,2,1,0:T(8,128)S(1)} %get-tuple-element.179, f32[4,768]{1,0:T(4,128)S(1)} %get-tuple-element.167, bf16[4,1,1,768,64]{3,4,2,1,0:T(8,128)(2,1)S(1)} %get-tuple-element.190, ...), kind=kOutput, calls=%fused_computation.7.clone.1 | convolution fusion | flops 309460992 | bytes 11132932 | tf_op jit(solution)/shard_map/while/body/eval_jaxpr/skgtr,skrd->skgtd/dot_general | solution.py:129
  150.0 1.6 fusion.115
  151.7 0.6 copy.54
  152.3 0.5 broadcast.437
  152.8 3.0 %reduce.15 = bf16[768,256]{1,0:T(8,128)(2,1)S(1)} reduce(bf16[768,1,256]{2,1,0:T(2,128)(2,1)S(1)} %bitcast.162, bf16[]{:T(256)} %broadcast.437), dimensions={1}, to_apply=%bitcast.124.reduce_sub_computation | reduce | bytes 786434
  155.9 0.8 reshape.683
  156.7 3.5 %all-to-all-start = ((bf16[4,2,24576]{2,1,0:T(2,128)(2,1)}), bf16[4,2,24576]{2,1,0:T(2,128)(2,1)S(1)}, u32[]{:S(2)}, u32[]{:S(2)}) async-start(bf16[4,2,24576]{2,1,0:T(2,128)(2,1)} %reshape.683), calls=%async_computation | async-start | bytes 786432 | tf_op jit(solution)/shard_map/all_to_all | solution.py:171
  160.2 9.1 %all_gather.21 = f32[2,2048]{1,0:T(2,128)S(1)} all-gather(f32[2,512]{1,0:T(2,128)S(1)} %get-tuple-element.89), channel_id=1, replica_groups=mesh['sp'=4,'tp'=4,'dp'=2] {'tp'}, dimensions={1}, use_global_device_ids=true | all-gather | bytes 20480 | tf_op jit(solution)/shard_map/all_gather | solution.py:86
  170.1 4.1 %fusion.30 = bf16[1,192,2048]{2,1,0:T(8,128)(2,1)} fusion(bf16[192,1024]{1,0:T(8,128)(2,1)S(1)} %bitcast.171, bf16[1024,2048]{1,0:T(8,128)(2,1)} %param.31, bf16[1,192,2048]{2,1,0:T(8,128)(2,1)S(1)} %copy-done.1, f32[2048]{0:T(1024)S(1)} %bitcast.174), kind=kOutput, calls=%fused_computation.32 | convolution fusion | flops 806879232 | bytes 6168576 | tf_op jit(solution)/shard_map/srq,qd->srd/dot_general | solution.py:169
  (88 shorter events, 4.7 us)
Async XLA Ops:
  6.5 1.0 copy-start
  6.5 45.7 %copy-start.4 = (bf16[2048,64]{0,1:T(8,128)(2,1)S(1)}, bf16[2048,64]{0,1:T(8,128)(2,1)}, u32[]{:S(2)}) copy-start(bf16[2048,64]{0,1:T(8,128)(2,1)} %param.26) | copy-start | bytes 786436
  6.5 46.0 %copy-start.3 = (bf16[2048,64]{0,1:T(8,128)(2,1)S(1)}, bf16[2048,64]{0,1:T(8,128)(2,1)}, u32[]{:S(2)}) copy-start(bf16[2048,64]{0,1:T(8,128)(2,1)} %param.27) | copy-start | bytes 786436
  6.5 46.3 %copy-start.7 = (bf16[64]{0:T(256)(128)(2,1)S(1)}, bf16[64]{0:T(256)(128)(2,1)}, u32[]{:S(2)}) copy-start(bf16[64]{0:T(256)(128)(2,1)} %param.29) | copy-start | bytes 388
  6.5 46.3 %copy-start.8 = (bf16[64]{0:T(256)(128)(2,1)S(1)}, bf16[64]{0:T(256)(128)(2,1)}, u32[]{:S(2)}) copy-start(bf16[64]{0:T(256)(128)(2,1)} %param.28) | copy-start | bytes 388
  6.5 46.3 %copy-start.2 = (bf16[1,128,2048]{2,1,0:T(8,128)(2,1)S(1)}, bf16[1,128,2048]{2,1,0:T(8,128)(2,1)}, u32[]{:S(2)}) copy-start(bf16[1,128,2048]{2,1,0:T(8,128)(2,1)} %param.20) | copy-start | bytes 1572868
  6.6 86.9 %all-gather.4.cloned.1.call-start = ((), (), s32[]{:S(2)}) async-start(), calls=%async_computation.1 | async-start | bytes 3932160 | tf_op jit(solution)/shard_map/all_gather | solution.py:96
  97.4 5.2 %copy-start.6 = (f32[4]{0:T(128)S(1)}, f32[4]{0:T(128)}, u32[]{:S(2)}) copy-start(f32[4]{0:T(128)} %param.30) | copy-start | bytes 52
  99.4 7.9 %collective-permute-start = (bf16[1,1,768,64]{2,3,1,0:T(8,128)(2,1)S(1)}, bf16[1,1,768,64]{2,3,1,0:T(8,128)(2,1)S(1)}, u32[]{:S(2)}, u32[]{:S(2)}) collective-permute-start(bf16[1,1,768,64]{2,3,1,0:T(8,128)(2,1)S(1)} %convert_element_type.131), channel_id=1, source_target_pairs={{0,8},{8,16},{16,24},{24,0},{1,9},{9,17},{17,25},{25,1},{2,10},{10... | collective-permute-start | bytes 294920 | tf_op jit(solution)/shard_map/ppermute | solution.py:150
  102.0 2.6 %copy-start.5 = (bf16[1,512,64]{1,2,0:T(8,128)(2,1)S(1)}, bf16[1,512,64]{1,2,0:T(8,128)(2,1)}, u32[]{:S(2)}) copy-start(bf16[1,512,64]{1,2,0:T(8,128)(2,1)} %all-gather) | copy-start | bytes 196612
  107.4 6.6 %collective-permute-start.1 = (bf16[1,1,768,64]{2,3,1,0:T(8,128)(2,1)S(1)}, bf16[1,1,768,64]{2,3,1,0:T(8,128)(2,1)}, u32[]{:S(2)}, u32[]{:S(2)}) collective-permute-start(bf16[1,1,768,64]{2,3,1,0:T(8,128)(2,1)S(1)} %collective-permute-done), channel_id=1, source_target_pairs={{0,8},{8,16},{16,24},{24,0},{1,9},{9,17},{17,25},{25,1},{2,10},{10... | collective-permute-start | bytes 294920 | tf_op jit(solution)/shard_map/ppermute | solution.py:150
  113.9 15.8 %collective-permute-start.2 = (bf16[1,1,768,64]{2,3,1,0:T(8,128)(2,1)}, bf16[1,1,768,64]{2,3,1,0:T(8,128)(2,1)S(1)}, u32[]{:S(2)}, u32[]{:S(2)}) collective-permute-start(bf16[1,1,768,64]{2,3,1,0:T(8,128)(2,1)} %collective-permute-done.1), channel_id=1, source_target_pairs={{0,8},{8,16},{16,24},{24,0},{1,9},{9,17},{17,25},{25,1},{2,10},{10... | collective-permute-start | bytes 294920 | tf_op jit(solution)/shard_map/ppermute | solution.py:150
  151.6 18.5 %copy-start.1 = (bf16[1,192,2048]{2,1,0:T(8,128)(2,1)S(1)}, bf16[1,192,2048]{2,1,0:T(8,128)(2,1)}, u32[]{:S(2)}) copy-start(bf16[1,192,2048]{2,1,0:T(8,128)(2,1)} %param.17) | copy-start | bytes 2359300
  156.7 12.5 %all-to-all-start = ((bf16[4,2,24576]{2,1,0:T(2,128)(2,1)}), bf16[4,2,24576]{2,1,0:T(2,128)(2,1)S(1)}, u32[]{:S(2)}, u32[]{:S(2)}) async-start(bf16[4,2,24576]{2,1,0:T(2,128)(2,1)} %reshape.683), calls=%async_computation | async-start | bytes 786432 | tf_op jit(solution)/shard_map/all_to_all | solution.py:171
Sparse Core Ops, SparseCore 0:
  52.3 41.0 all-gather.3
